TPU v7x, 32 devices: a whole 2x2x4 slice. The times are simulated.
32 devices in a mesh: fs: 8 (over z, x), tp: 4 (over y, core).
Axes of the slice: x: 2, y: 2, z: 4, core: 2. Of those that a mesh axis runs over, the one named last changes fastest.
Arguments:
- tokens: bfloat16 [1024, 2048], P('fs', 'tp'), may hold values from -6 to 6
- routes: int32 [1024, 2], P('fs'), may hold values from 0 to 3, all different within a row; in each aligned block of 128 rows (0 to 127, 128 to 255, ...) at most 96 rows name the same one
- route_weight: float32 [1024, 2], P('fs'), may hold values from 0.1 to 1
- norm_gain: float32 [2048], P('fs'), may hold values from 0.1 to 1.9
- expert_gate: float32 [4, 2048, 512], P(None, 'fs', 'tp'), may hold values from -0.125 to 0.125
- expert_up: float32 [4, 2048, 512], P(None, 'fs', 'tp'), may hold values from -0.125 to 0.125
- expert_down: float32 [4, 2048, 512], P(None, 'fs', 'tp'), may hold values from -0.25 to 0.25
- shared_gate: float32 [2048, 512], P('fs', 'tp'), may hold values from -0.125 to 0.125
- shared_up: float32 [2048, 512], P('fs', 'tp'), may hold values from -0.125 to 0.125
- shared_down: float32 [512, 2048], P('tp', 'fs'), may hold values from -0.25 to 0.25
Outputs:
- mixed: bfloat16 [1024, 2048], P('fs', 'tp')
- gate_sampler: bfloat16 [8, 2048, 256], P('fs', None, 'tp')
- up_sampler: bfloat16 [8, 2048, 256], P('fs', None, 'tp')
- down_sampler: bfloat16 [8, 2048, 256], P('fs', 'tp')
- shared_gate_out: bfloat16 [2048, 512], P(None, 'tp')
- shared_up_out: bfloat16 [2048, 512], P(None, 'tp')
- shared_down_out: bfloat16 [512, 2048], P('tp')
Inputs may be any that keep to these rules, and one draw needn't show every extreme that they name: `routes`: each row names 2 different experts. In each aligned block of 128 rows no expert is named by more than 96 rows, a bound that some block reaches.
All inputs are finite; a program needn't handle non-finite values.
Results may differ from a plain program's by a relative error of at most 0.009.
Values may be sent and summed in bfloat16 or wider, within the bound.
No kernel may reach another device: no remote copies, remote signals or barrier semaphores. Data moves between devices by JAX's collectives and lax.ppermute only.
A program may use at most 64 MiB of HBM per device.

v0:
```python
import jax
import jax.numpy as jnp
from jax import lax
from jax.sharding import PartitionSpec as P

EPS = 1e-06


def to_owners(matrix, expert_count, unit_count):
    row_share = matrix.shape[1]
    return (
        matrix.reshape(expert_count, row_share, 2, unit_count)
        .transpose(0, 2, 1, 3)
        .reshape(2 * expert_count, row_share, unit_count)
    )


def on_device(
    tokens,
    routes,
    route_weight,
    norm_gain,
    expert_gate,
    expert_up,
    expert_down,
    shared_gate,
    shared_up,
    shared_down,
):
    fs_count = lax.axis_size("fs")
    tp_count = lax.axis_size("tp")
    expert_count, row_share, col_share = expert_gate.shape
    unit_count = col_share // 2
    model_width = row_share * fs_count
    quarter = model_width // tp_count
    tok_count, pick_count = routes.shape
    capacity = 2 * ((3 * tok_count * pick_count + 4 * expert_count - 1) // (4 * expert_count))
    slot_count = fs_count * capacity
    row_gain = norm_gain[None, :, None]
    gate_owned = to_owners((expert_gate * row_gain).astype(jnp.bfloat16), expert_count, unit_count)
    up_owned = to_owners((expert_up * row_gain).astype(jnp.bfloat16), expert_count, unit_count)
    gate_new, up_new = (
        lax.all_to_all(gate_owned, "fs", split_axis=0, concat_axis=1, tiled=True),
        lax.all_to_all(up_owned, "fs", split_axis=0, concat_axis=1, tiled=True),
    )
    down_owned = to_owners(expert_down.astype(jnp.bfloat16), expert_count, unit_count)
    down_new = lax.all_to_all(
        lax.all_to_all(down_owned, "fs", split_axis=0, concat_axis=1, tiled=True),
        "tp",
        split_axis=1,
        concat_axis=2,
        tiled=True,
    )
    shared_gate_new, shared_up_new, shared_down_new = (
        lax.all_gather(
            (shared_gate * norm_gain[:, None]).astype(jnp.bfloat16), "fs", axis=0, tiled=True
        ),
        lax.all_gather(
            (shared_up * norm_gain[:, None]).astype(jnp.bfloat16), "fs", axis=0, tiled=True
        ),
        lax.all_gather(shared_down.astype(jnp.bfloat16), "fs", axis=1, tiled=True),
    )
    gathered = lax.all_gather(tokens, "tp", axis=1, tiled=True)
    tokens_wide = gathered.astype(jnp.float32)
    normed = (
        tokens_wide * lax.rsqrt(jnp.mean(tokens_wide * tokens_wide, axis=1, keepdims=True) + EPS)
    ).astype(jnp.bfloat16)
    shared_act = jnp.dot(normed, shared_gate_new, preferred_element_type=jnp.float32)
    shared_lin = jnp.dot(normed, shared_up_new, preferred_element_type=jnp.float32)
    shared_hidden = (jax.nn.silu(shared_act) * shared_lin).astype(jnp.bfloat16)
    shared_term = jnp.dot(shared_hidden, shared_down_new, preferred_element_type=jnp.float32)
    shared_sum = lax.psum_scatter(
        shared_term.astype(jnp.bfloat16), "tp", scatter_dimension=1, tiled=True
    ).astype(jnp.float32)
    assigned = routes.reshape(-1)
    onehot = (assigned[:, None] == jnp.arange(expert_count, dtype=jnp.int32)[None, :]).astype(
        jnp.int32
    )
    earlier = jnp.cumsum(onehot, axis=0) - onehot
    position = jnp.sum(earlier * onehot, axis=1)
    slot_index = assigned * capacity + position
    token_index = jnp.arange(tok_count * pick_count, dtype=jnp.int32) // pick_count
    slot_token = (
        jnp.full((expert_count * capacity,), tok_count, jnp.int32).at[slot_index].set(token_index)
    )
    padded = jnp.concatenate([normed, jnp.zeros((1, model_width), jnp.bfloat16)], axis=0)
    own_part = lax.dynamic_slice_in_dim(padded, lax.axis_index("tp") * quarter, quarter, 1)
    outgoing = jnp.repeat(
        own_part[slot_token].reshape(expert_count, capacity, quarter), 2, axis=0
    ).reshape(slot_count, quarter)
    arrived = lax.all_to_all(outgoing, "fs", split_axis=0, concat_axis=0, tiled=True)
    portion = lax.all_gather(arrived, "tp", axis=1, tiled=True)
    gate_rows = gate_new[0]
    up_rows = up_new[0]
    gate_act = jnp.dot(portion, gate_rows, preferred_element_type=jnp.float32)
    up_act = jnp.dot(portion, up_rows, preferred_element_type=jnp.float32)
    hidden = (jax.nn.silu(gate_act) * up_act).astype(jnp.bfloat16)
    down_cols = down_new[0]
    half_sum = lax.dot_general(
        lax.all_gather(hidden, "tp", axis=1, tiled=True),
        down_cols,
        (((1,), (1,)), ((), ())),
        preferred_element_type=jnp.float32,
    )
    returned = lax.all_to_all(
        half_sum.astype(jnp.bfloat16), "fs", split_axis=0, concat_axis=0, tiled=True
    )
    pair_sum = jnp.sum(
        returned.astype(jnp.float32).reshape(expert_count, 2, capacity, quarter), axis=1
    ).reshape(expert_count * capacity, quarter)
    gathered_slots = pair_sum[slot_index].reshape(tok_count, pick_count, quarter)
    routed = jnp.sum(gathered_slots * route_weight[:, :, None], axis=1)
    mixed = (shared_sum + routed).astype(jnp.bfloat16)
    return (mixed, gate_new, up_new, down_new, shared_gate_new, shared_up_new, shared_down_new)


def solution(mesh):
    in_specs = (
        P("fs", "tp"),
        P("fs", None),
        P("fs", None),
        P("fs"),
        P(None, "fs", "tp"),
        P(None, "fs", "tp"),
        P(None, "fs", "tp"),
        P("fs", "tp"),
        P("fs", "tp"),
        P("tp", "fs"),
    )
    out_specs = (
        P("fs", "tp"),
        P("fs", None, "tp"),
        P("fs", None, "tp"),
        P("fs", "tp", None),
        P(None, "tp"),
        P(None, "tp"),
        P("tp", None),
    )
    return jax.shard_map(
        on_device, mesh=mesh, in_specs=in_specs, out_specs=out_specs, check_vma=False
    )
```

profile of v0, /device:TPU:0, one launch (start us, length us, event | category | flops | bytes accessed | tf_op | source)
XLA Modules:
  0.0 257.9 jit_solution(7877371888522557811)
XLA Ops:
  7.2 0.8 copy.45
  8.0 0.1 eq.29
  8.1 0.1 eq.25
  8.3 0.7 broadcast_multiply_fusion
  9.0 8.9 %all_gather.18 = bf16[128,2048]{1,0:T(8,128)(2,1)S(1)} all-gather(bf16[128,512]{1,0:T(8,128)(2,1)} %param.10), channel_id=1, replica_groups=mesh['fs'=8,'tp'=4] {'tp'}, dimensions={1}, use_global_device_ids=true | all-gather | bytes 655360 | tf_op jit(solution)/shard_map/all_gather | solution.py:63
  17.8 0.2 fusion.2
  18.0 0.2 fusion.3
  18.2 1.2 reduce-window.6
  19.5 0.1 copy.47
  19.8 0.1 copy.44
  20.0 0.1 mul.94
  20.1 1.4 scatter_custom_fusion
  21.6 2.1 gather_fusion
  23.8 26.3 %all_to_all.75 = bf16[8,96,512]{2,1,0:T(8,128)(2,1)} all-to-all(bf16[8,96,512]{2,1,0:T(8,128)(2,1)S(1)} %bitcast.62), channel_id=1, replica_groups=mesh['fs'=8,'tp'=4] {'fs'}, dimensions={0} | all-to-all | bytes 1572864 | tf_op jit(solution)/shard_map/all_to_all | solution.py:91
  50.2 0.2 multiply_convert_fusion.1
  50.3 0.2 fusion.17
  50.6 0.1 pad_maximum_fusion
  50.7 0.9 copy.50
  51.6 3.6 %all-to-all-start.1 = ((bf16[8,256,64]{1,2,0:T(8,128)(2,1)}), bf16[8,256,64]{1,2,0:T(8,128)(2,1)S(1)}, u32[]{:S(2)}, u32[]{:S(2)}) async-start(bf16[8,256,64]{1,2,0:T(8,128)(2,1)} %copy.50), calls=%async_computation.2 | async-start | bytes 524288 | tf_op jit(solution)/shard_map/all_to_all | solution.py:43
  55.3 0.1 fusion.16
  55.4 0.1 pad_maximum_fusion.2
  55.5 0.9 copy.56
  56.4 7.8 %all-to-all-done.1 = bf16[8,256,64]{1,2,0:T(8,128)(2,1)S(1)} async-done(((bf16[8,256,64]{1,2,0:T(8,128)(2,1)}), bf16[8,256,64]{1,2,0:T(8,128)(2,1)S(1)}, u32[]{:S(2)}, u32[]{:S(2)}) %all-to-all-start.1) | async-done | bytes 262176 | tf_op jit(solution)/shard_map/all_to_all | solution.py:43
  64.2 3.6 %all-to-all-start.3 = ((bf16[8,256,64]{1,2,0:T(8,128)(2,1)}), bf16[8,256,64]{1,2,0:T(8,128)(2,1)S(1)}, u32[]{:S(2)}, u32[]{:S(2)}) async-start(bf16[8,256,64]{1,2,0:T(8,128)(2,1)} %copy.56), calls=%async_computation.4 | async-start | bytes 524288 | tf_op jit(solution)/shard_map/all_to_all | solution.py:48
  67.8 0.1 pad_maximum_fusion.1
  67.9 0.9 copy.53
  68.8 7.6 %all-to-all-done.3 = bf16[8,256,64]{1,2,0:T(8,128)(2,1)S(1)} async-done(((bf16[8,256,64]{1,2,0:T(8,128)(2,1)}), bf16[8,256,64]{1,2,0:T(8,128)(2,1)S(1)}, u32[]{:S(2)}, u32[]{:S(2)}) %all-to-all-start.3) | async-done | bytes 262176 | tf_op jit(solution)/shard_map/all_to_all | solution.py:48
  76.4 3.6 %all-to-all-start.2 = ((bf16[8,256,64]{1,2,0:T(8,128)(2,1)}), bf16[8,256,64]{1,2,0:T(8,128)(2,1)S(1)}, u32[]{:S(2)}, u32[]{:S(2)}) async-start(bf16[8,256,64]{1,2,0:T(8,128)(2,1)} %copy.53), calls=%async_computation.3 | async-start | bytes 524288 | tf_op jit(solution)/shard_map/all_to_all | solution.py:44
  80.1 33.5 %all_gather.19 = bf16[2048,128]{1,0:T(8,128)(2,1)S(1)} all-gather(bf16[256,128]{1,0:T(8,128)(2,1)S(1)} %get-tuple-element.34), channel_id=1, replica_groups=mesh['fs'=8,'tp'=4] {'fs'}, dimensions={0}, use_global_device_ids=true | all-gather | bytes 589824 | tf_op jit(solution)/shard_map/all_gather | solution.py:55
  113.6 0.3 copy.72
  113.9 0.3 reshape.148
  114.2 0.5 broadcast.90
  114.7 11.5 %reduce = bf16[2048,64]{1,0:T(8,128)(2,1)S(1)} reduce(bf16[2048,1,64]{2,1,0:T(2,128)(2,1)S(1)} %bitcast.60, bf16[]{:T(256)} %broadcast.90), dimensions={1}, to_apply=%bitcast.45.reduce_sub_computation | reduce | bytes 524290
  126.2 1.1 reshape.151
  127.3 3.4 %all-to-all-start.4 = ((bf16[4,2,16384]{2,1,0:T(2,128)(2,1)}), bf16[4,2,16384]{2,1,0:T(2,128)(2,1)S(1)}, u32[]{:S(2)}, u32[]{:S(2)}) async-start(bf16[4,2,16384]{2,1,0:T(2,128)(2,1)} %reshape.151), calls=%async_computation.5 | async-start | bytes 524288 | tf_op jit(solution)/shard_map/all_to_all | solution.py:47
  130.8 31.5 %all_gather.20 = bf16[2048,128]{1,0:T(8,128)(2,1)S(1)} all-gather(bf16[256,128]{1,0:T(8,128)(2,1)S(1)} %get-tuple-element.35), channel_id=1, replica_groups=mesh['fs'=8,'tp'=4] {'fs'}, dimensions={0}, use_global_device_ids=true | all-gather | bytes 589824 | tf_op jit(solution)/shard_map/all_gather | solution.py:58
  162.3 0.7 copy.74
  163.0 0.7 copy.75
  163.7 0.6 reshape.152
  164.4 0.6 copy.59
  165.0 0.2 all_to_all.62
  165.3 3.1 %fusion.20 = f32[768,64]{0,1:T(8,128)S(1)} fusion(bf16[768,2048]{1,0:T(8,128)(2,1)} %all-gather.2.cloned.1.call-done, bf16[2048,64]{0,1:T(8,128)(2,1)} %bitcast.71), kind=kOutput, calls=%fused_computation.54 | convolution fusion | flops 201326592 | bytes 3604480 | tf_op jit(solution)/shard_map/dot_general | solution.py:95
  168.4 1.1 fusion
  169.5 7.3 %all_gather.23 = bf16[768,256]{0,1:T(8,128)(2,1)S(1)} all-gather(bf16[768,64]{0,1:T(8,128)(2,1)S(1)} %fusion), channel_id=1, replica_groups=mesh['fs'=8,'tp'=4] {'tp'}, dimensions={1}, use_global_device_ids=true | all-gather | bytes 491520 | tf_op jit(solution)/shard_map/all_gather | solution.py:100
  176.7 1.3 convolution_convert_fusion.1
  178.0 4.3 %all-to-all-start.5 = ((bf16[8,96,512]{2,1,0:T(8,128)(2,1)}), bf16[8,96,512]{2,1,0:T(8,128)(2,1)}, u32[]{:S(2)}, u32[]{:S(2)}) async-start(bf16[8,96,512]{2,1,0:T(8,128)(2,1)} %bitcast.12), calls=%async_computation.6 | async-start | bytes 1572864 | tf_op jit(solution)/shard_map/all_to_all | solution.py:105
  182.4 43.3 %all_gather.21 = bf16[128,2048]{1,0:T(8,128)(2,1)S(1)} all-gather(bf16[128,256]{1,0:T(8,128)(2,1)S(1)} %convert_element_type.61), channel_id=1, replica_groups=mesh['fs'=8,'tp'=4] {'fs'}, dimensions={1}, use_global_device_ids=true | all-gather | bytes 589824 | tf_op jit(solution)/shard_map/all_gather | solution.py:61
  225.7 0.3 fusion.19
  226.0 1.3 convolution_convert_fusion
  227.4 0.1 copy.61
  227.5 0.2 copy.51
  227.7 0.8 all_to_all.66
  228.5 0.1 copy.54
  228.6 0.8 all_to_all.67
  229.5 0.8 copy.65
  230.3 1.4 convert_reduce_fusion
  231.7 1.0 gather_fusion.1
  232.6 0.3 reshape.121
  233.0 0.7 multiply_reduce_fusion
  233.7 13.4 %reduce-scatter.2.cloned.1.call-done = bf16[128,512]{1,0:T(8,128)(2,1)} async-done(((bf16[128,2048]{1,0:T(8,128)(2,1)}), bf16[128,512]{1,0:T(8,128)(2,1)}) %reduce-scatter.2.cloned.1.call-update) | async-done | bytes 131088 | tf_op jit(solution)/shard_map/reduce_scatter | solution.py:72
  247.1 1.6 add_convert_fusion
  248.7 0.8 copy.81
  249.5 0.8 copy.82
  250.3 0.8 copy.83
  (47 shorter events, 0.8 us)
Async XLA Ops:
  7.2 158.1 %all-gather.2.cloned.1.call-start = ((), (), s32[]{:S(2)}) async-start(), calls=%async_computation.8 | async-start | bytes 3932160 | tf_op jit(solution)/shard_map/all_gather | solution.py:92
  21.6 28.5 %copy-start.2 = (f32[4,256,128]{2,1,0:T(8,128)S(1)}, f32[4,256,128]{2,1,0:T(8,128)}, u32[]{:S(2)}) copy-start(f32[4,256,128]{2,1,0:T(8,128)} %param.14) | copy-start | bytes 1572868
  21.6 28.5 %copy-start.3 = (f32[4,256,128]{2,1,0:T(8,128)S(1)}, f32[4,256,128]{2,1,0:T(8,128)}, u32[]{:S(2)}) copy-start(f32[4,256,128]{2,1,0:T(8,128)} %param.15) | copy-start | bytes 1572868
  21.6 28.5 %copy-start.8 = (f32[256]{0:T(256)S(1)}, f32[256]{0:T(256)}, u32[]{:S(2)}) copy-start(f32[256]{0:T(256)} %param.13) | copy-start | bytes 3076
  50.1 5.1 %copy-start.1 = (f32[4,256,128]{2,1,0:T(8,128)S(1)}, f32[4,256,128]{2,1,0:T(8,128)}, u32[]{:S(2)}) copy-start(f32[4,256,128]{2,1,0:T(8,128)} %param.16) | copy-start | bytes 1572868
  51.6 12.6 %all-to-all-start.1 = ((bf16[8,256,64]{1,2,0:T(8,128)(2,1)}), bf16[8,256,64]{1,2,0:T(8,128)(2,1)S(1)}, u32[]{:S(2)}, u32[]{:S(2)}) async-start(bf16[8,256,64]{1,2,0:T(8,128)(2,1)} %copy.50), calls=%async_computation.2 | async-start | bytes 524288 | tf_op jit(solution)/shard_map/all_to_all | solution.py:43
  55.2 13.6 %copy-start.7 = (f32[128,256]{1,0:T(8,128)S(1)}, f32[128,256]{1,0:T(8,128)}, u32[]{:S(2)}) copy-start(f32[128,256]{1,0:T(8,128)} %param.19) | copy-start | bytes 393220
  55.3 24.8 %copy-start.5 = (f32[256,128]{1,0:T(8,128)S(1)}, f32[256,128]{1,0:T(8,128)}, u32[]{:S(2)}) copy-start(f32[256,128]{1,0:T(8,128)} %param.17) | copy-start | bytes 393220
  55.3 24.7 %copy-start.6 = (f32[256,128]{1,0:T(8,128)S(1)}, f32[256,128]{1,0:T(8,128)}, u32[]{:S(2)}) copy-start(f32[256,128]{1,0:T(8,128)} %param.18) | copy-start | bytes 393220
  64.2 12.2 %all-to-all-start.3 = ((bf16[8,256,64]{1,2,0:T(8,128)(2,1)}), bf16[8,256,64]{1,2,0:T(8,128)(2,1)S(1)}, u32[]{:S(2)}, u32[]{:S(2)}) async-start(bf16[8,256,64]{1,2,0:T(8,128)(2,1)} %copy.56), calls=%async_computation.4 | async-start | bytes 524288 | tf_op jit(solution)/shard_map/all_to_all | solution.py:48
  76.4 50.9 %all-to-all-start.2 = ((bf16[8,256,64]{1,2,0:T(8,128)(2,1)}), bf16[8,256,64]{1,2,0:T(8,128)(2,1)S(1)}, u32[]{:S(2)}, u32[]{:S(2)}) async-start(bf16[8,256,64]{1,2,0:T(8,128)(2,1)} %copy.53), calls=%async_computation.3 | async-start | bytes 524288 | tf_op jit(solution)/shard_map/all_to_all | solution.py:44
  127.3 36.4 %all-to-all-start.4 = ((bf16[4,2,16384]{2,1,0:T(2,128)(2,1)}), bf16[4,2,16384]{2,1,0:T(2,128)(2,1)S(1)}, u32[]{:S(2)}, u32[]{:S(2)}) async-start(bf16[4,2,16384]{2,1,0:T(2,128)(2,1)} %reshape.151), calls=%async_computation.5 | async-start | bytes 524288 | tf_op jit(solution)/shard_map/all_to_all | solution.py:47
  165.0 3.4 %copy-start.4 = (bf16[8,8,8,256]{3,2,0,1:T(8,128)(2,1)S(1)}, bf16[8,8,8,256]{3,2,0,1:T(8,128)(2,1)}, u32[]{:S(2)}) copy-start(bf16[8,8,8,256]{3,2,0,1:T(8,128)(2,1)} %copy.75) | copy-start | bytes 786436
  165.2 3.1 %copy-start = (bf16[768,2048]{1,0:T(8,128)(2,1)S(1)}, bf16[768,2048]{1,0:T(8,128)(2,1)}, u32[]{:S(2)}) copy-start(bf16[768,2048]{1,0:T(8,128)(2,1)} %all-gather.2.cloned.1.call-done) | copy-start | bytes 9437188
  178.0 49.4 %copy-start.9 = (f32[128,2]{0,1:T(2,128)S(1)}, f32[128,2]{0,1:T(2,128)}, u32[]{:S(2)}) copy-start(f32[128,2]{0,1:T(2,128)} %param.12) | copy-start | bytes 3076
  178.0 52.3 %all-to-all-start.5 = ((bf16[8,96,512]{2,1,0:T(8,128)(2,1)}), bf16[8,96,512]{2,1,0:T(8,128)(2,1)}, u32[]{:S(2)}, u32[]{:S(2)}) async-start(bf16[8,96,512]{2,1,0:T(8,128)(2,1)} %bitcast.12), calls=%async_computation.6 | async-start | bytes 1572864 | tf_op jit(solution)/shard_map/all_to_all | solution.py:105
  182.4 64.7 %reduce-scatter.2.cloned.1.call-start = ((), (), s32[]{:S(2)}) async-start(), calls=%async_computation.7 | async-start | bytes 655360 | tf_op jit(solution)/shard_map/reduce_scatter | solution.py:72
Sparse Core Ops, SparseCore 0:
  50.2 27.1 all-gather.1
  227.5 19.5 reduce-scatter.1
where the time goes:
time: 259 us; the launch traced here: 258 us
  blocking collectives  151 us (58%)
  waiting for transfers between devices  28.8 us (11%)
  local copies, waits for them, and re-layouts  19.9 us (8%)
  starting transfers between devices  18.7 us (7%)
  other arithmetic  18.2 us (7%)
  between operations  14.4 us (6%)
  matrix products  7.12 us (3%)
    all_gather x1, blocking collectives, on_device(): lax.all_gather(shared_down.astype(jnp.bfloat16), 'fs', axis=1, tiled=True)  43.3 us
    all_gather x1, blocking collectives, on_device(): lax.all_gather((shared_gate * norm_gain[:, None]).astype(jnp.bfloat16), '...  33.5 us
    all_gather x1, blocking collectives, on_device(): lax.all_gather((shared_up * norm_gain[:, None]).astype(jnp.bfloat16), 'fs...  31.5 us
    all_to_all x1, blocking collectives, on_device(): lax.all_to_all(outgoing, 'fs', split_axis=0, concat_axis=0, tiled=True)  26.3 us
    reduce_scatter x1, waiting for transfers between devices, on_device(): lax.psum_scatter(shared_term.astype(jnp.bfloat16), 'tp', scatter_dimensio...  13.4 us
    unnamed x2, other arithmetic  11.6 us
    all_gather x1, blocking collectives, on_device(): gathered = lax.all_gather(tokens, 'tp', axis=1, tiled=True)  8.87 us
    all_to_all x1, waiting for transfers between devices, on_device(): lax.all_to_all(gate_owned, 'fs', split_axis=0, concat_axis=1, tiled=True)  7.75 us
  transfers between devices with their start and end apart: 7, of which 3 were waited for; matrix products, arithmetic and copies ran while one was open for 10% of the time, Pallas kernels for 0%

commit v1 on v0

--- a/solution.py
+++ b/solution.py
@@ -44,12 +44,20 @@
         lax.all_to_all(up_owned, "fs", split_axis=0, concat_axis=1, tiled=True),
     )
     down_owned = to_owners(expert_down.astype(jnp.bfloat16), expert_count, unit_count)
-    down_new = lax.all_to_all(
-        lax.all_to_all(down_owned, "fs", split_axis=0, concat_axis=1, tiled=True),
-        "tp",
-        split_axis=1,
-        concat_axis=2,
-        tiled=True,
+    down_new = jnp.concatenate(
+        lax.all_to_all(
+            jnp.stack(
+                jnp.split(
+                    lax.all_to_all(down_owned, "fs", split_axis=0, concat_axis=1, tiled=True),
+                    lax.axis_size("tp"),
+                    axis=1,
+                )
+            ),
+            "tp",
+            0,
+            0,
+        ),
+        axis=2,
     )
     shared_gate_new, shared_up_new, shared_down_new = (
         lax.all_gather(

time: 259 us -> 243 us (0.938)
  other arithmetic: 18.2 us -> 7.43 us
  local copies, waits for them, and re-layouts: 19.9 us -> 15.1 us
    unnamed x2 -> x1, other arithmetic: 11.6 us -> 0.07 us
    all_to_all x1, waiting for transfers between devices: 7.58 us -> 0.01 us  [on_device(): lax.all_to_all(down_owned, 'fs', split_axis=0, concat_axis=1, tiled=True)]
    all_to_all x1, waiting for transfers between devices: 0.01 us -> 7.31 us  [on_device(): lax.all_to_all(up_owned, 'fs', split_axis=0, concat_axis=1, tiled=True)]
    unnamed x29 -> x24, local copies, waits for them, and re-layouts: 6.41 us -> 4.17 us
  transfers between devices with their start and end apart: 7 -> 7, of which waited for: 3 -> 3; matrix products, arithmetic and copies ran while one was open for 10% -> 6% of each run, Pallas kernels for 0% -> 0%
where the time goes in v1:
time: 243 us; the launch traced here: 242 us
  blocking collectives  151 us (62%)
  waiting for transfers between devices  28.9 us (12%)
  starting transfers between devices  18.7 us (8%)
  local copies, waits for them, and re-layouts  15.1 us (6%)
  between operations  14.4 us (6%)
  other arithmetic  7.43 us (3%)
  matrix products  7.1 us (3%)
    all_gather x1, blocking collectives, on_device(): lax.all_gather(shared_down.astype(jnp.bfloat16), 'fs', axis=1, tiled=True)  43.3 us
    all_gather x1, blocking collectives, on_device(): lax.all_gather((shared_gate * norm_gain[:, None]).astype(jnp.bfloat16), '...  33.7 us
    all_gather x1, blocking collectives, on_device(): lax.all_gather((shared_up * norm_gain[:, None]).astype(jnp.bfloat16), 'fs...  31.5 us
    all_to_all x1, blocking collectives, on_device(): lax.all_to_all(outgoing, 'fs', split_axis=0, concat_axis=0, tiled=True)  26.3 us
    reduce_scatter x1, waiting for transfers between devices, on_device(): lax.psum_scatter(shared_term.astype(jnp.bfloat16), 'tp', scatter_dimensio...  13.6 us
    all_gather x1, blocking collectives, on_device(): gathered = lax.all_gather(tokens, 'tp', axis=1, tiled=True)  8.87 us
    all_to_all x1, waiting for transfers between devices, on_device(): lax.all_to_all(gate_owned, 'fs', split_axis=0, concat_axis=1, tiled=True)  7.91 us
    all_to_all x1, waiting for transfers between devices, on_device(): lax.all_to_all(up_owned, 'fs', split_axis=0, concat_axis=1, tiled=True)  7.31 us
  transfers between devices with their start and end apart: 7, of which 3 were waited for; matrix products, arithmetic and copies ran while one was open for 6% of the time, Pallas kernels for 0%

profile of v1, /device:TPU:0, one launch (start us, length us, event | category | flops | bytes accessed | tf_op | source)
XLA Modules:
  0.0 242.2 jit_solution(6645416624748768437)
XLA Ops:
  7.2 0.0 all-gather.2.cloned.1.call-start
  7.2 0.8 copy.44
  8.0 0.1 eq.29
  8.1 0.1 eq.25
  8.3 0.7 broadcast_multiply_fusion
  9.0 8.9 %all_gather.18 = bf16[128,2048]{1,0:T(8,128)(2,1)S(1)} all-gather(bf16[128,512]{1,0:T(8,128)(2,1)} %param.10), channel_id=1, replica_groups=mesh['fs'=8,'tp'=4] {'tp'}, dimensions={1}, use_global_device_ids=true | all-gather | bytes 655360 | tf_op jit(solution)/shard_map/all_gather | solution.py:71
  17.8 0.2 fusion.2
  18.0 0.2 fusion.3
  18.2 1.2 reduce-window.6
  19.4 0.1 slice.36
  19.5 0.1 copy.46
  19.7 0.1 copy.47
  19.8 0.1 add_bitcast_fusion
  19.8 0.1 copy.43
  20.0 0.1 mul.94
  20.1 1.4 scatter_custom_fusion
  21.6 2.1 gather_fusion
  23.7 0.1 broadcast_in_dim.8
  23.8 26.3 %all_to_all.62 = bf16[8,96,512]{2,1,0:T(8,128)(2,1)} all-to-all(bf16[8,96,512]{2,1,0:T(8,128)(2,1)S(1)} %bitcast.68), channel_id=1, replica_groups=mesh['fs'=8,'tp'=4] {'fs'}, dimensions={0} | all-to-all | bytes 1572864 | tf_op jit(solution)/shard_map/all_to_all | solution.py:99
  50.1 0.2 multiply_convert_fusion.1
  50.3 0.2 fusion.17
  50.6 0.1 pad_maximum_fusion
  50.7 0.9 copy.49
  51.6 3.6 %all-to-all-start.1 = ((bf16[8,256,64]{1,2,0:T(8,128)(2,1)}), bf16[8,256,64]{1,2,0:T(8,128)(2,1)S(1)}, u32[]{:S(2)}, u32[]{:S(2)}) async-start(bf16[8,256,64]{1,2,0:T(8,128)(2,1)} %copy.49), calls=%async_computation.2 | async-start | bytes 524288 | tf_op jit(solution)/shard_map/all_to_all | solution.py:43
  55.2 0.1 pad_maximum_fusion.1
  55.3 0.9 copy.52
  56.3 7.9 %all-to-all-done.1 = bf16[8,256,64]{1,2,0:T(8,128)(2,1)S(1)} async-done(((bf16[8,256,64]{1,2,0:T(8,128)(2,1)}), bf16[8,256,64]{1,2,0:T(8,128)(2,1)S(1)}, u32[]{:S(2)}, u32[]{:S(2)}) %all-to-all-start.1) | async-done | bytes 262176 | tf_op jit(solution)/shard_map/all_to_all | solution.py:43
  64.2 3.6 %all-to-all-start.2 = ((bf16[8,256,64]{1,2,0:T(8,128)(2,1)}), bf16[8,256,64]{1,2,0:T(8,128)(2,1)S(1)}, u32[]{:S(2)}, u32[]{:S(2)}) async-start(bf16[8,256,64]{1,2,0:T(8,128)(2,1)} %copy.52), calls=%async_computation.3 | async-start | bytes 524288 | tf_op jit(solution)/shard_map/all_to_all | solution.py:44
  67.8 0.1 fusion.16
  68.0 0.1 pad_maximum_fusion.2
  68.1 0.9 copy.55
  69.0 0.1 multiply_convert_fusion.3
  69.1 7.3 %all-to-all-done.2 = bf16[8,256,64]{1,2,0:T(8,128)(2,1)S(1)} async-done(((bf16[8,256,64]{1,2,0:T(8,128)(2,1)}), bf16[8,256,64]{1,2,0:T(8,128)(2,1)S(1)}, u32[]{:S(2)}, u32[]{:S(2)}) %all-to-all-start.2) | async-done | bytes 262176 | tf_op jit(solution)/shard_map/all_to_all | solution.py:44
  76.4 3.6 %all-to-all-start.3 = ((bf16[8,256,64]{1,2,0:T(8,128)(2,1)}), bf16[8,256,64]{1,2,0:T(8,128)(2,1)S(1)}, u32[]{:S(2)}, u32[]{:S(2)}) async-start(bf16[8,256,64]{1,2,0:T(8,128)(2,1)} %copy.55), calls=%async_computation.4 | async-start | bytes 524288 | tf_op jit(solution)/shard_map/all_to_all | solution.py:51
  80.0 33.7 %all_gather.19 = bf16[2048,128]{1,0:T(8,128)(2,1)S(1)} all-gather(bf16[256,128]{1,0:T(8,128)(2,1)S(1)} %get-tuple-element.38), channel_id=1, replica_groups=mesh['fs'=8,'tp'=4] {'fs'}, dimensions={0}, use_global_device_ids=true | all-gather | bytes 589824 | tf_op jit(solution)/shard_map/all_gather | solution.py:63
  113.7 31.5 %all_gather.20 = bf16[2048,128]{1,0:T(8,128)(2,1)S(1)} all-gather(bf16[256,128]{1,0:T(8,128)(2,1)S(1)} %get-tuple-element.39), channel_id=1, replica_groups=mesh['fs'=8,'tp'=4] {'fs'}, dimensions={0}, use_global_device_ids=true | all-gather | bytes 589824 | tf_op jit(solution)/shard_map/all_gather | solution.py:66
  145.2 0.2 copy.56
  145.4 0.1 all_to_all.50
  145.5 0.7 pad_maximum_fusion.3
  146.3 3.4 %all-to-all-start.4 = ((bf16[4,1,512,64]{2,3,1,0:T(8,128)(2,1)}), bf16[4,1,512,64]{2,3,1,0:T(8,128)(2,1)S(1)}, u32[]{:S(2)}, u32[]{:S(2)}) async-start(bf16[4,1,512,64]{2,3,1,0:T(8,128)(2,1)} %pad_maximum_fusion.3), calls=%async_computation.5 | async-start | bytes 524288 | tf_op jit(solution)/shard_map/all_to_all | solution.py:48
  149.7 3.1 %fusion.20 = f32[768,64]{0,1:T(8,128)S(1)} fusion(bf16[768,2048]{1,0:T(8,128)(2,1)} %all-gather.2.cloned.1.call-done, bf16[2048,64]{0,1:T(8,128)(2,1)S(1)} %bitcast.77), kind=kOutput, calls=%fused_computation.59 | convolution fusion | flops 201326592 | bytes 3604480 | tf_op jit(solution)/shard_map/dot_general | solution.py:103
  152.9 1.1 fusion
  153.9 6.9 %all_gather.23 = bf16[768,256]{0,1:T(8,128)(2,1)S(1)} all-gather(bf16[768,64]{0,1:T(8,128)(2,1)S(1)} %fusion), channel_id=1, replica_groups=mesh['fs'=8,'tp'=4] {'tp'}, dimensions={1}, use_global_device_ids=true | all-gather | bytes 491520 | tf_op jit(solution)/shard_map/all_gather | solution.py:108
  160.9 1.3 convolution_convert_fusion.1
  162.2 4.3 %all-to-all-start.5 = ((bf16[8,96,512]{2,1,0:T(8,128)(2,1)}), bf16[8,96,512]{2,1,0:T(8,128)(2,1)}, u32[]{:S(2)}, u32[]{:S(2)}) async-start(bf16[8,96,512]{2,1,0:T(8,128)(2,1)} %bitcast.16), calls=%async_computation.6 | async-start | bytes 1572864 | tf_op jit(solution)/shard_map/all_to_all | solution.py:113
  166.5 0.0 reduce-scatter.2.cloned.1.call-start
  166.6 43.3 %all_gather.21 = bf16[128,2048]{1,0:T(8,128)(2,1)S(1)} all-gather(bf16[128,256]{1,0:T(8,128)(2,1)S(1)} %convert_element_type.61), channel_id=1, replica_groups=mesh['fs'=8,'tp'=4] {'fs'}, dimensions={1}, use_global_device_ids=true | all-gather | bytes 589824 | tf_op jit(solution)/shard_map/all_gather | solution.py:69
  209.9 0.3 fusion.19
  210.2 1.3 convolution_convert_fusion
  211.5 0.1 copy.57
  211.6 0.2 copy.50
  211.8 0.8 all_to_all.54
  212.6 0.1 copy.53
  212.8 0.8 all_to_all.55
  213.6 0.8 copy.60
  214.5 1.4 convert_reduce_fusion
  215.8 1.0 gather_fusion.1
  216.8 0.3 reshape.127
  217.1 0.7 multiply_reduce_fusion
  217.8 13.6 %reduce-scatter.2.cloned.1.call-done = bf16[128,512]{1,0:T(8,128)(2,1)} async-done(((bf16[128,2048]{1,0:T(8,128)(2,1)}), bf16[128,512]{1,0:T(8,128)(2,1)}) %reduce-scatter.2.cloned.1.call-update) | async-done | bytes 131088 | tf_op jit(solution)/shard_map/reduce_scatter | solution.py:80
  231.4 1.6 add_convert_fusion
  233.0 0.8 copy.74
  233.8 0.8 copy.75
  234.6 0.8 copy.76
  (40 shorter events, 0.3 us)
Async XLA Ops:
  7.2 142.5 %all-gather.2.cloned.1.call-start = ((), (), s32[]{:S(2)}) async-start(), calls=%async_computation.8 | async-start | bytes 3932160 | tf_op jit(solution)/shard_map/all_gather | solution.py:100
  21.6 28.5 %copy-start.2 = (f32[4,256,128]{2,1,0:T(8,128)S(1)}, f32[4,256,128]{2,1,0:T(8,128)}, u32[]{:S(2)}) copy-start(f32[4,256,128]{2,1,0:T(8,128)} %param.14) | copy-start | bytes 1572868
  21.6 28.5 %copy-start.3 = (f32[4,256,128]{2,1,0:T(8,128)S(1)}, f32[4,256,128]{2,1,0:T(8,128)}, u32[]{:S(2)}) copy-start(f32[4,256,128]{2,1,0:T(8,128)} %param.15) | copy-start | bytes 1572868
  21.6 28.5 %copy-start.7 = (f32[256]{0:T(256)S(1)}, f32[256]{0:T(256)}, u32[]{:S(2)}) copy-start(f32[256]{0:T(256)} %param.13) | copy-start | bytes 3076
  50.3 5.9 %copy-start.1 = (f32[4,256,128]{2,1,0:T(8,128)S(1)}, f32[4,256,128]{2,1,0:T(8,128)}, u32[]{:S(2)}) copy-start(f32[4,256,128]{2,1,0:T(8,128)} %param.16) | copy-start | bytes 1572868
  51.6 12.6 %all-to-all-start.1 = ((bf16[8,256,64]{1,2,0:T(8,128)(2,1)}), bf16[8,256,64]{1,2,0:T(8,128)(2,1)S(1)}, u32[]{:S(2)}, u32[]{:S(2)}) async-start(bf16[8,256,64]{1,2,0:T(8,128)(2,1)} %copy.49), calls=%async_computation.2 | async-start | bytes 524288 | tf_op jit(solution)/shard_map/all_to_all | solution.py:43
  55.2 13.8 %copy-start.6 = (f32[128,256]{1,0:T(8,128)S(1)}, f32[128,256]{1,0:T(8,128)}, u32[]{:S(2)}) copy-start(f32[128,256]{1,0:T(8,128)} %param.19) | copy-start | bytes 393220
  55.2 13.8 %copy-start.4 = (f32[256,128]{1,0:T(8,128)S(1)}, f32[256,128]{1,0:T(8,128)}, u32[]{:S(2)}) copy-start(f32[256,128]{1,0:T(8,128)} %param.17) | copy-start | bytes 393220
  55.2 13.8 %copy-start.5 = (f32[256,128]{1,0:T(8,128)S(1)}, f32[256,128]{1,0:T(8,128)}, u32[]{:S(2)}) copy-start(f32[256,128]{1,0:T(8,128)} %param.18) | copy-start | bytes 393220
  64.2 12.2 %all-to-all-start.2 = ((bf16[8,256,64]{1,2,0:T(8,128)(2,1)}), bf16[8,256,64]{1,2,0:T(8,128)(2,1)S(1)}, u32[]{:S(2)}, u32[]{:S(2)}) async-start(bf16[8,256,64]{1,2,0:T(8,128)(2,1)} %copy.52), calls=%async_computation.3 | async-start | bytes 524288 | tf_op jit(solution)/shard_map/all_to_all | solution.py:44
  76.4 68.8 %all-to-all-start.3 = ((bf16[8,256,64]{1,2,0:T(8,128)(2,1)}), bf16[8,256,64]{1,2,0:T(8,128)(2,1)S(1)}, u32[]{:S(2)}, u32[]{:S(2)}) async-start(bf16[8,256,64]{1,2,0:T(8,128)(2,1)} %copy.55), calls=%async_computation.4 | async-start | bytes 524288 | tf_op jit(solution)/shard_map/all_to_all | solution.py:51
  146.3 14.6 %all-to-all-start.4 = ((bf16[4,1,512,64]{2,3,1,0:T(8,128)(2,1)}), bf16[4,1,512,64]{2,3,1,0:T(8,128)(2,1)S(1)}, u32[]{:S(2)}, u32[]{:S(2)}) async-start(bf16[4,1,512,64]{2,3,1,0:T(8,128)(2,1)} %pad_maximum_fusion.3), calls=%async_computation.5 | async-start | bytes 524288 | tf_op jit(solution)/shard_map/all_to_all | solution.py:48
  149.7 3.1 %copy-start = (bf16[768,2048]{1,0:T(8,128)(2,1)S(1)}, bf16[768,2048]{1,0:T(8,128)(2,1)}, u32[]{:S(2)}) copy-start(bf16[768,2048]{1,0:T(8,128)(2,1)} %all-gather.2.cloned.1.call-done) | copy-start | bytes 9437188
  162.2 49.4 %copy-start.8 = (f32[128,2]{0,1:T(2,128)S(1)}, f32[128,2]{0,1:T(2,128)}, u32[]{:S(2)}) copy-start(f32[128,2]{0,1:T(2,128)} %param.12) | copy-start | bytes 3076
  162.2 52.3 %all-to-all-start.5 = ((bf16[8,96,512]{2,1,0:T(8,128)(2,1)}), bf16[8,96,512]{2,1,0:T(8,128)(2,1)}, u32[]{:S(2)}, u32[]{:S(2)}) async-start(bf16[8,96,512]{2,1,0:T(8,128)(2,1)} %bitcast.16), calls=%async_computation.6 | async-start | bytes 1572864 | tf_op jit(solution)/shard_map/all_to_all | solution.py:113
  166.5 64.9 %reduce-scatter.2.cloned.1.call-start = ((), (), s32[]{:S(2)}) async-start(), calls=%async_computation.7 | async-start | bytes 655360 | tf_op jit(solution)/shard_map/reduce_scatter | solution.py:80
Sparse Core Ops, SparseCore 0:
  50.2 27.1 all-gather.1
  211.6 19.7 reduce-scatter.1
